TPU v7x, 32 devices: a whole 2x2x4 slice. The times are simulated.
32 devices in a mesh: grp: 2 (over y), fs: 4 (over z), tp: 4 (over x, core).
Axes of the slice: x: 2, y: 2, z: 4, core: 2. Of those that a mesh axis runs over, the one named last changes fastest.
Arguments:
- tokens: bfloat16 [1536, 2048], P(('grp', 'tp')), parts along dimension 0, may hold values from -6 to 6
- routes: int32 [1536, 2], P(('grp', 'tp')), parts along dimension 0, may hold values from 0 to 3, all different within a row; in each aligned block of 192 rows (0 to 191, 192 to 383, ...) at most 128 rows name the same one
- route_weight: float32 [1536, 2], P(('grp', 'tp')), parts along dimension 0, may hold values from 0.2 to 1
- norm_gain: float32 [2048], P('fs'), may hold values from 0.1 to 1.9
- gate_train: float32 [4, 2048, 5632], P('tp', 'fs'), may hold values from -0.125 to 0.125
- up_train: float32 [4, 2048, 5632], P('tp', 'fs'), may hold values from -0.125 to 0.125
- down_train: float32 [4, 5632, 2048], P('tp', None, 'fs'), may hold values from -0.109375 to 0.109375
Outputs:
- gate_serve: bfloat16 [8, 2048, 5632], P(('grp', 'tp'), None, 'fs'), parts along dimension 0
- up_serve: bfloat16 [8, 2048, 5632], P(('grp', 'tp'), None, 'fs'), parts along dimension 0
- down_serve: bfloat16 [8, 5632, 2048], P(('grp', 'tp'), 'fs'), parts along dimension 0
- mixed: bfloat16 [1536, 2048], P(('grp', 'tp'), 'fs'), parts along dimension 0
There are 2 independent parts, one for each index of `grp`. A program takes and returns all parts, laid end to end along the dimension named above; an argument that names none is the same for every part. Nothing has to cross between parts.
Inputs may be any that keep to these rules, and one draw needn't show every extreme that they name: `routes`: each row names 2 different experts. In each aligned block of 192 rows no expert is named by more than 128 rows, a bound that some block reaches.
All inputs are finite; a program needn't handle non-finite values.
Results may differ from a plain program's by a relative error of at most 0.0087.
Values may be sent and summed in bfloat16 or wider, within the bound.
A program may use at most 128 MiB of HBM per device.

v0:
```python
import jax
import jax.numpy as jnp
from jax import lax
from jax.sharding import PartitionSpec as P

EXPERTS = 4
CAP = 128


def shards(tokens, routes, route_weight, norm_gain, gate_train, up_train, down_train):
    fs_count = lax.axis_size("fs")
    pieces = min(fs_count, 32)
    copies = fs_count // pieces
    gain_column = norm_gain[:, None]
    gate_low = (gate_train[0] * gain_column).astype(jnp.bfloat16)
    up_low = (up_train[0] * gain_column).astype(jnp.bfloat16)
    down_low = down_train[0].astype(jnp.bfloat16)
    gate_wide = jnp.tile(gate_low, (1, copies))
    up_wide = jnp.tile(up_low, (1, copies))
    down_wide = jnp.tile(down_low, (copies, 1))
    gate_new, up_new = (
        lax.all_to_all(gate_wide, "fs", split_axis=1, concat_axis=0, tiled=True),
        lax.all_to_all(up_wide, "fs", split_axis=1, concat_axis=0, tiled=True),
    )
    down_new = lax.all_to_all(down_wide, "fs", split_axis=0, concat_axis=1, tiled=True)
    tok_float = tokens.astype(jnp.float32)
    normed = (
        tok_float * lax.rsqrt(jnp.mean(tok_float * tok_float, axis=-1, keepdims=True) + 1e-06)
    ).astype(jnp.bfloat16)
    chosen = routes.reshape(-1)
    chosen_hot = (chosen[:, None] == jnp.arange(EXPERTS, dtype=jnp.int32)[None, :]).astype(
        jnp.int32
    )
    before = jnp.cumsum(chosen_hot, axis=0) - chosen_hot
    slot_rank = jnp.sum(before * chosen_hot, axis=1)
    slot_index = (chosen * CAP + slot_rank).reshape(routes.shape)
    slot_range = jnp.arange(EXPERTS * CAP, dtype=jnp.int32)
    select_rows = jnp.any(slot_range[:, None, None] == slot_index[None, :, :], axis=-1).astype(
        jnp.bfloat16
    )
    outgoing = jnp.dot(select_rows, normed, preferred_element_type=jnp.float32).astype(jnp.bfloat16)
    outgoing = outgoing.reshape(EXPERTS, CAP, normed.shape[1])
    arrived = lax.all_to_all(outgoing, "tp", split_axis=0, concat_axis=0, tiled=True).reshape(
        EXPERTS * CAP, normed.shape[1]
    )
    slot_count = EXPERTS * CAP // copies
    copy_index = lax.axis_index("fs") // pieces
    my_rows = lax.dynamic_slice_in_dim(arrived, copy_index * slot_count, slot_count, 0)
    gated = jnp.dot(my_rows, gate_new, preferred_element_type=jnp.float32)
    lifted = jnp.dot(my_rows, up_new, preferred_element_type=jnp.float32)
    hidden = (jax.nn.silu(gated) * lifted).astype(jnp.bfloat16)
    partial_out = jnp.dot(hidden, down_new, preferred_element_type=jnp.float32)
    placed = jnp.zeros((EXPERTS * CAP, partial_out.shape[1]), jnp.float32)
    placed = lax.dynamic_update_slice_in_dim(placed, partial_out, copy_index * slot_count, 0)
    expert_out = lax.psum_scatter(placed, "fs", scatter_dimension=1, tiled=True).astype(
        jnp.bfloat16
    )
    returned = lax.all_to_all(
        expert_out.reshape(EXPERTS, CAP, expert_out.shape[1]),
        "tp",
        split_axis=0,
        concat_axis=0,
        tiled=True,
    )
    returned = returned.reshape(EXPERTS * CAP, expert_out.shape[1]).astype(jnp.float32)
    blend_weight = jnp.sum(
        jnp.where(
            slot_range[None, None, :] == slot_index[:, :, None], route_weight[:, :, None], 0.0
        ),
        axis=1,
    )
    mixed = jnp.dot(
        blend_weight, returned, precision=lax.Precision.HIGHEST, preferred_element_type=jnp.float32
    )
    return (gate_new[None], up_new[None], down_new[None], mixed.astype(jnp.bfloat16))


def solution(mesh):
    in_specs = (
        P(("grp", "tp"), None),
        P(("grp", "tp"), None),
        P(("grp", "tp"), None),
        P("fs"),
        P("tp", "fs", None),
        P("tp", "fs", None),
        P("tp", None, "fs"),
    )
    out_specs = (
        P(("grp", "tp"), None, "fs"),
        P(("grp", "tp"), None, "fs"),
        P(("grp", "tp"), "fs", None),
        P(("grp", "tp"), "fs"),
    )
    return jax.shard_map(shards, mesh=mesh, in_specs=in_specs, out_specs=out_specs, check_vma=False)
```

profile of v0, /device:TPU:0, one launch (start us, length us, event | category | flops | bytes accessed | tf_op | source)
XLA Modules:
  0.0 587.4 jit_solution(4837379173826643466)
XLA Ops:
  7.2 0.8 copy.54
  8.0 0.1 eq.56
  8.1 0.1 eq.52
  8.3 1.2 reduce-window.6
  9.5 0.2 slice_reduce_fusion
  9.7 0.2 reduce-window.9
  9.9 0.1 add_bitcast_fusion
  10.0 0.1 reduce_sum.30
  10.1 0.1 copy.56
  10.2 0.7 multiply_add_fusion
  10.9 0.1 fusion.7
  11.1 1.4 fusion.3
  12.4 3.3 convolution_convert_fusion
  15.7 4.2 all-to-all-start.3
  19.9 14.5 %squeeze.7 = f32[512,4,1408]{2,1,0:T(4,128)} reshape(f32[1,512,5632]{2,1,0:T(8,128)} %param.11) | data formatting | bytes 23068672 | tf_op jit(solution)/shard_map/squeeze | solution.py:15
  34.5 0.0 copy-start
  34.5 14.5 %squeeze.8 = f32[512,4,1408]{2,1,0:T(4,128)} reshape(f32[1,512,5632]{2,1,0:T(8,128)} %param.12) | data formatting | bytes 23068672 | tf_op jit(solution)/shard_map/squeeze | solution.py:16
  49.0 0.0 copy-done
  49.0 16.8 %fusion = (bf16[512,4,1408]{2,0,1:T(8,128)(2,1)}, bf16[512,4,1408]{2,0,1:T(8,128)(2,1)}) fusion(f32[512,4,1408]{2,1,0:T(4,128)} %squeeze.8, f32[512]{0:T(512)S(1)} %copy-done, f32[512,4,1408]{2,1,0:T(4,128)} %squeeze.7), kind=kLoop, calls=%fused_computation.1 | loop fusion | flops 11534336 | bytes 34605056 | tf_op jit(solution)/shard_map/convert_element_type | solution.py:16
  65.8 0.0 all-to-all-done.3
  65.9 5.7 all-to-all-start
  71.6 7.5 %convert_element_type.44 = bf16[1,5632,512]{2,1,0:T(8,128)(2,1)} convert(f32[1,5632,512]{2,1,0:T(8,128)} %param.13) | non-fusion elementwise | flops 2883584 | bytes 17301504 | tf_op jit(solution)/shard_map/convert_element_type | solution.py:17
  79.1 120.5 %all-to-all-done = bf16[512,4,1408]{2,0,1:T(8,128)(2,1)} async-done(((bf16[512,4,1408]{2,0,1:T(8,128)(2,1)}), bf16[512,4,1408]{2,0,1:T(8,128)(2,1)}, u32[]{:S(2)}, u32[]{:S(2)}) %all-to-all-start) | async-done | bytes 5767200 | tf_op jit(solution)/shard_map/all_to_all | solution.py:22
  199.6 133.5 %all_to_all.58 = bf16[4,1408,512]{2,1,0:T(8,128)(2,1)} all-to-all(bf16[4,1408,512]{2,1,0:T(8,128)(2,1)} %bitcast.49), channel_id=1, replica_groups=mesh['grp'=2,'fs'=4,'tp'=4] {'fs'}, dimensions={0} | all-to-all | bytes 11534336 | tf_op jit(solution)/shard_map/all_to_all | solution.py:25
  333.2 5.2 all-to-all-start.1
  338.3 0.2 reduce-scatter.2.cloned.1.call-start
  338.6 8.3 %copy.53 = bf16[4,1408,512]{1,2,0:T(8,128)(2,1)} copy(bf16[4,1408,512]{2,1,0:T(8,128)(2,1)} %all_to_all.58) | data formatting | bytes 11534336 | tf_op jit(solution)/shard_map/all_to_all | solution.py:25
  346.9 7.6 %fusion.14 = f32[512,1408]{1,0:T(8,128)} fusion(bf16[512,2048]{1,0:T(8,128)(2,1)S(1)} %bitcast.50, bf16[2048,1408]{1,0:T(8,128)(2,1)} %bitcast.10), kind=kOutput, calls=%fused_computation.30 | convolution fusion | flops 2952790016 | bytes 10747904 | tf_op jit(solution)/shard_map/dot_general | solution.py:49
  354.5 110.3 %all-to-all-done.1 = bf16[512,4,1408]{2,0,1:T(8,128)(2,1)} async-done(((bf16[512,4,1408]{2,0,1:T(8,128)(2,1)}), bf16[512,4,1408]{2,0,1:T(8,128)(2,1)}, u32[]{:S(2)}, u32[]{:S(2)}) %all-to-all-start.1) | async-done | bytes 5767200 | tf_op jit(solution)/shard_map/all_to_all | solution.py:23
  464.8 13.9 %fusion.8 = f32[512,2048]{1,0:T(8,128)} fusion(bf16[1408,2048]{0,1:T(8,128)(2,1)} %bitcast.47, bf16[512,2048]{1,0:T(8,128)(2,1)S(1)} %bitcast.51, bf16[2048,1408]{1,0:T(8,128)(2,1)} %bitcast.11, f32[512,1408]{1,0:T(8,128)} %fusion.14), kind=kOutput, calls=%fused_computation.17 | convolution fusion | flops 5909905408 | bytes 20709376 | tf_op jit(solution)/shard_map/dot_general | solution.py:52
  478.7 0.0 copy-start.1
  478.7 0.0 reduce-scatter.2.cloned.1.call-update
  478.7 75.2 %reduce-scatter.2.cloned.1.call-done = f32[512,512]{1,0:T(8,128)} async-done(((f32[512,2048]{1,0:T(8,128)}), f32[512,512]{1,0:T(8,128)}) %reduce-scatter.2.cloned.1.call-update) | async-done | bytes 1048592 | tf_op jit(solution)/shard_map/reduce_scatter | solution.py:55
  553.9 2.1 convert_element_type.52
  555.9 3.5 all-to-all-start.4
  559.4 0.0 copy-done.1
  559.4 0.2 select_reduce_fusion
  559.6 8.2 %copy.57 = bf16[1,1408,2048]{2,1,0:T(8,128)(2,1)} copy(bf16[1,1408,2048]{1,2,0:T(8,128)(2,1)} %bitcast.48) | data formatting | bytes 11534336
  567.9 0.3 all-to-all-done.4
  568.2 1.2 convolution_convert_fusion.1
  569.4 5.6 copy.68
  575.0 5.6 copy.69
  (3 shorter events, 0.0 us)
Async XLA Ops:
  15.7 50.1 %all-to-all-start.3 = ((bf16[4,128,2048]{2,1,0:T(8,128)(2,1)}), bf16[4,128,2048]{2,1,0:T(8,128)(2,1)S(1)}, u32[]{:S(2)}, u32[]{:S(2)}) async-start(bf16[4,128,2048]{2,1,0:T(8,128)(2,1)} %bitcast.8), calls=%async_computation.3 | async-start | bytes 4194304 | tf_op jit(solution)/shard_map/all_to_all | solution.py:43
  34.5 14.5 %copy-start = (f32[512]{0:T(512)S(1)}, f32[512]{0:T(512)}, u32[]{:S(2)}) copy-start(f32[512]{0:T(512)} %param.10) | copy-start | bytes 6148
  65.9 133.8 %all-to-all-start = ((bf16[512,4,1408]{2,0,1:T(8,128)(2,1)}), bf16[512,4,1408]{2,0,1:T(8,128)(2,1)}, u32[]{:S(2)}, u32[]{:S(2)}) async-start(bf16[512,4,1408]{2,0,1:T(8,128)(2,1)} %get-tuple-element.17), calls=%async_computation | async-start | bytes 11534336 | tf_op jit(solution)/shard_map/all_to_all | solution.py:22
  333.2 131.6 %all-to-all-start.1 = ((bf16[512,4,1408]{2,0,1:T(8,128)(2,1)}), bf16[512,4,1408]{2,0,1:T(8,128)(2,1)}, u32[]{:S(2)}, u32[]{:S(2)}) async-start(bf16[512,4,1408]{2,0,1:T(8,128)(2,1)} %get-tuple-element.16), calls=%async_computation.1 | async-start | bytes 11534336 | tf_op jit(solution)/shard_map/all_to_all | solution.py:23
  338.3 215.5 %reduce-scatter.2.cloned.1.call-start = ((), (), s32[]{:S(2)}) async-start(), calls=%async_computation.6 | async-start | bytes 5242880 | tf_op jit(solution)/shard_map/reduce_scatter | solution.py:55
  478.7 80.8 %copy-start.1 = (f32[192,2]{0,1:T(2,128)S(1)}, f32[192,2]{0,1:T(2,128)}, u32[]{:S(2)}) copy-start(f32[192,2]{0,1:T(2,128)} %param.9) | copy-start | bytes 4612
  555.9 12.3 %all-to-all-start.4 = ((bf16[4,128,512]{2,1,0:T(8,128)(2,1)}), bf16[4,128,512]{2,1,0:T(8,128)(2,1)S(1)}, u32[]{:S(2)}, u32[]{:S(2)}) async-start(bf16[4,128,512]{2,1,0:T(8,128)(2,1)} %bitcast.13), calls=%async_computation.5 | async-start | bytes 1048576 | tf_op jit(solution)/shard_map/all_to_all | solution.py:58
Sparse Core Ops, SparseCore 0:
  478.8 74.9 reduce-scatter.1
where the time goes:
time: 589 us; the launch traced here: 587 us
  waiting for transfers between devices  306 us (52%)
  blocking collectives  134 us (23%)
  local copies, waits for them, and re-layouts  58.3 us (10%)
  other arithmetic  30.4 us (5%)
  matrix products  25.9 us (4%)
  starting transfers between devices  18.8 us (3%)
  between operations  14.1 us (2%)
    all_to_all x1, blocking collectives, shards(): lax.all_to_all(down_wide, 'fs', split_axis=0, concat_axis=1, tiled=True)  134 us
    all_to_all x1, waiting for transfers between devices, shards(): lax.all_to_all(gate_wide, 'fs', split_axis=1, concat_axis=0, tiled=True)  120 us
    all_to_all x1, waiting for transfers between devices, shards(): lax.all_to_all(up_wide, 'fs', split_axis=1, concat_axis=0, tiled=True)  110 us
    reduce_scatter x1, waiting for transfers between devices, shards(): lax.psum_scatter(placed, 'fs', scatter_dimension=1, tiled=True)  75.2 us
    unnamed x8, local copies, waits for them, and re-layouts  20.2 us
    convert_element_type x1, other arithmetic, shards(): up_low = (up_train[0] * gain_column).astype(jnp.bfloat16)  16.8 us
    squeeze x1, local copies, waits for them, and re-layouts, shards(): gate_low = (gate_train[0] * gain_column).astype(jnp.bfloat16)  14.5 us
    squeeze x1, local copies, waits for them, and re-layouts, shards(): up_low = (up_train[0] * gain_column).astype(jnp.bfloat16)  14.5 us
  transfers between devices with their start and end apart: 5, of which 4 were waited for; matrix products, arithmetic and copies ran while one was open for 13% of the time, Pallas kernels for 0%

commit v1 on v0

--- a/solution.py
+++ b/solution.py
@@ -5,6 +5,12 @@
 
 EXPERTS = 4
 CAP = 128
+
+
+def exchange_blocks(shard, name, split, join):
+    cells = jnp.split(shard, lax.axis_size(name), axis=split)
+    got = lax.all_to_all(jnp.stack(cells), name, 0, 0)
+    return jnp.concatenate(got, axis=join)
 
 
 def shards(tokens, routes, route_weight, norm_gain, gate_train, up_train, down_train):
@@ -20,7 +26,7 @@
     down_wide = jnp.tile(down_low, (copies, 1))
     gate_new, up_new = (
         lax.all_to_all(gate_wide, "fs", split_axis=1, concat_axis=0, tiled=True),
-        lax.all_to_all(up_wide, "fs", split_axis=1, concat_axis=0, tiled=True),
+        exchange_blocks(up_wide, "fs", 1, 0),
     )
     down_new = lax.all_to_all(down_wide, "fs", split_axis=0, concat_axis=1, tiled=True)
     tok_float = tokens.astype(jnp.float32)

time: 589 us -> 566 us (0.961)
  blocking collectives: 134 us -> 0 us
  waiting for transfers between devices: 306 us -> 426 us
  local copies, waits for them, and re-layouts: 58.3 us -> 44.2 us
    all_to_all x1 -> x0, blocking collectives: 134 us -> none  [shards(): lax.all_to_all(down_wide, 'fs', split_axis=0, concat_axis=1, tiled=True)]
    all_to_all x1 -> x2, waiting for transfers between devices: 110 us -> 227 us  [the longest x1 117 us: shards(): lax.all_to_all(down_wide, 'fs', split_axis=0, concat_axis=1, tiled=True)]
    squeeze x1 -> x0, local copies, waits for them, and re-layouts: 14.5 us -> none  [shards(): up_low = (up_train[0] * gain_column).astype(jnp.bfloat16)]
    convert_element_type x1, other arithmetic: 16.8 us -> 5.8 us  [shards(): up_low = (up_train[0] * gain_column).astype(jnp.bfloat16)]
    convert_element_type x0 -> x1, other arithmetic: none -> 8.06 us  [shards(): gate_low = (gate_train[0] * gain_column).astype(jnp.bfloat16)]
  transfers between devices with their start and end apart: 5 -> 6, of which waited for: 4 -> 6; matrix products, arithmetic and copies ran while one was open for 13% -> 11% of each run, Pallas kernels for 0% -> 0%
where the time goes in v1:
time: 566 us; the launch traced here: 564 us
  waiting for transfers between devices  426 us (75%)
  local copies, waits for them, and re-layouts  44.2 us (8%)
  other arithmetic  30.6 us (5%)
  matrix products  25.9 us (5%)
  starting transfers between devices  23.9 us (4%)
  between operations  14.1 us (2%)
    all_to_all x1, waiting for transfers between devices, shards(): lax.all_to_all(gate_wide, 'fs', split_axis=1, concat_axis=0, tiled=True)  120 us
    all_to_all x1, waiting for transfers between devices, shards(): lax.all_to_all(down_wide, 'fs', split_axis=0, concat_axis=1, tiled=True)  117 us
    all_to_all x1, waiting for transfers between devices, exchange_blocks(): got = lax.all_to_all(jnp.stack(cells), name, 0, 0)  110 us
    reduce_scatter x1, waiting for transfers between devices, shards(): lax.psum_scatter(placed, 'fs', scatter_dimension=1, tiled=True)  75.4 us
    unnamed x8, local copies, waits for them, and re-layouts  20.2 us
    squeeze x1, local copies, waits for them, and re-layouts, shards(): gate_low = (gate_train[0] * gain_column).astype(jnp.bfloat16)  14.5 us
    dot_general x1, matrix products, shards(): partial_out = jnp.dot(hidden, down_new, preferred_element_type=jnp.float32)  13.9 us
  transfers between devices with their start and end apart: 6, of which 6 were waited for; matrix products, arithmetic and copies ran while one was open for 11% of the time, Pallas kernels for 0%

profile of v1, /device:TPU:0, one launch (start us, length us, event | category | flops | bytes accessed | tf_op | source)
XLA Modules:
  0.0 564.4 jit_solution(9464458475550337377)
XLA Ops:
  7.2 0.8 copy.48
  8.0 0.1 eq.56
  8.1 0.1 eq.52
  8.3 1.2 reduce-window.6
  9.5 0.2 slice_reduce_fusion
  9.7 0.2 reduce-window.9
  9.9 0.1 add_bitcast_fusion
  10.0 0.1 reduce_sum.30
  10.1 0.1 copy.50
  10.2 0.7 multiply_add_fusion
  10.9 0.1 fusion.7
  11.1 1.4 fusion.3
  12.4 3.3 convolution_convert_fusion
  15.7 4.2 all-to-all-start.3
  19.9 0.0 copy-start
  20.0 14.5 %squeeze.7 = f32[512,4,1408]{2,1,0:T(4,128)} reshape(f32[1,512,5632]{2,1,0:T(8,128)} %param.11) | data formatting | bytes 23068672 | tf_op jit(solution)/shard_map/squeeze | solution.py:21
  34.5 0.0 copy-done
  34.5 8.1 %fusion.1 = bf16[512,4,1408]{2,0,1:T(8,128)(2,1)} fusion(f32[512,4,1408]{2,1,0:T(4,128)} %squeeze.7, f32[512]{0:T(512)S(1)} %copy-done), kind=kLoop, calls=%fused_computation.3 | loop fusion | flops 5767168 | bytes 17303552 | tf_op jit(solution)/shard_map/convert_element_type | solution.py:21
  42.5 3.1 all-to-all-done.3
  45.6 5.7 %all-to-all-start = ((bf16[512,4,1408]{2,0,1:T(8,128)(2,1)}), bf16[512,4,1408]{2,0,1:T(8,128)(2,1)}, u32[]{:S(2)}, u32[]{:S(2)}) async-start(bf16[512,4,1408]{2,0,1:T(8,128)(2,1)} %fusion.1), calls=%async_computation | async-start | bytes 11534336 | tf_op jit(solution)/shard_map/all_to_all | solution.py:28
  51.3 7.5 %convert_element_type.43 = bf16[1,5632,512]{2,1,0:T(8,128)(2,1)} convert(f32[1,5632,512]{2,1,0:T(8,128)} %param.13) | non-fusion elementwise | flops 2883584 | bytes 17301504 | tf_op jit(solution)/shard_map/convert_element_type | solution.py:23
  58.9 119.6 %all-to-all-done = bf16[512,4,1408]{2,0,1:T(8,128)(2,1)} async-done(((bf16[512,4,1408]{2,0,1:T(8,128)(2,1)}), bf16[512,4,1408]{2,0,1:T(8,128)(2,1)}, u32[]{:S(2)}, u32[]{:S(2)}) %all-to-all-start) | async-done | bytes 5767200 | tf_op jit(solution)/shard_map/all_to_all | solution.py:28
  178.4 5.2 all-to-all-start.2
  183.6 5.8 %fusion = bf16[512,5632]{1,0:T(8,128)(2,1)S(1)} fusion(f32[1,512,5632]{2,1,0:T(8,128)} %param.12, f32[512]{0:T(512)S(1)} %copy-done), kind=kLoop, calls=%fused_computation.1 | loop fusion | flops 5767168 | bytes 17303552 | tf_op jit(solution)/shard_map/convert_element_type | solution.py:22
  189.4 0.4 slice_bitcast_fusion.3
  189.9 3.2 pad_maximum_fusion
  193.1 116.8 %all-to-all-done.2 = bf16[4,1408,512]{2,1,0:T(8,128)(2,1)} async-done(((bf16[4,1408,512]{2,1,0:T(8,128)(2,1)}), bf16[4,1408,512]{2,1,0:T(8,128)(2,1)}, u32[]{:S(2)}, u32[]{:S(2)}) %all-to-all-start.2) | async-done | bytes 5767200 | tf_op jit(solution)/shard_map/all_to_all | solution.py:31
  309.9 5.2 all-to-all-start.1
  315.1 0.2 reduce-scatter.2.cloned.1.call-start
  315.3 8.3 %copy.47 = bf16[4,1408,512]{1,2,0:T(8,128)(2,1)} copy(bf16[4,1408,512]{2,1,0:T(8,128)(2,1)} %all-to-all-done.2) | data formatting | bytes 11534336 | tf_op jit(solution)/shard_map/all_to_all | solution.py:31
  323.7 7.6 %fusion.14 = f32[512,1408]{1,0:T(8,128)} fusion(bf16[512,2048]{1,0:T(8,128)(2,1)S(1)} %bitcast.59, bf16[2048,1408]{1,0:T(8,128)(2,1)} %bitcast.14), kind=kOutput, calls=%fused_computation.35 | convolution fusion | flops 2952790016 | bytes 10747904 | tf_op jit(solution)/shard_map/dot_general | solution.py:55
  331.3 110.3 %all-to-all-done.1 = bf16[4,512,1408]{2,1,0:T(8,128)(2,1)} async-done(((bf16[4,512,1408]{2,1,0:T(8,128)(2,1)}), bf16[4,512,1408]{2,1,0:T(8,128)(2,1)}, u32[]{:S(2)}, u32[]{:S(2)}) %all-to-all-start.1) | async-done | bytes 5767200 | tf_op jit(solution)/shard_map/all_to_all | solution.py:12
  441.6 13.9 %fusion.8 = f32[512,2048]{1,0:T(8,128)} fusion(bf16[1408,2048]{0,1:T(8,128)(2,1)} %bitcast.56, bf16[512,2048]{1,0:T(8,128)(2,1)S(1)} %bitcast.60, bf16[2048,1408]{1,0:T(8,128)(2,1)} %bitcast.15, f32[512,1408]{1,0:T(8,128)} %fusion.14), kind=kOutput, calls=%fused_computation.22 | convolution fusion | flops 5909905408 | bytes 20709376 | tf_op jit(solution)/shard_map/dot_general | solution.py:58
  455.4 0.0 copy-start.1
  455.5 0.0 reduce-scatter.2.cloned.1.call-update
  455.5 75.4 %reduce-scatter.2.cloned.1.call-done = f32[512,512]{1,0:T(8,128)} async-done(((f32[512,2048]{1,0:T(8,128)}), f32[512,512]{1,0:T(8,128)}) %reduce-scatter.2.cloned.1.call-update) | async-done | bytes 1048592 | tf_op jit(solution)/shard_map/reduce_scatter | solution.py:61
  530.9 2.1 convert_element_type.51
  533.0 3.5 all-to-all-start.4
  536.5 0.0 copy-done.1
  536.5 0.2 select_reduce_fusion
  536.7 8.2 %copy.51 = bf16[1,1408,2048]{2,1,0:T(8,128)(2,1)} copy(bf16[1,1408,2048]{1,2,0:T(8,128)(2,1)} %bitcast.57) | data formatting | bytes 11534336
  544.9 0.3 all-to-all-done.4
  545.3 1.2 convolution_convert_fusion.1
  546.4 5.6 copy.59
  552.0 5.6 copy.60
  (3 shorter events, 0.0 us)
Async XLA Ops:
  15.7 29.9 %all-to-all-start.3 = ((bf16[4,128,2048]{2,1,0:T(8,128)(2,1)}), bf16[4,128,2048]{2,1,0:T(8,128)(2,1)S(1)}, u32[]{:S(2)}, u32[]{:S(2)}) async-start(bf16[4,128,2048]{2,1,0:T(8,128)(2,1)} %bitcast.12), calls=%async_computation.3 | async-start | bytes 4194304 | tf_op jit(solution)/shard_map/all_to_all | solution.py:49
  19.9 14.5 %copy-start = (f32[512]{0:T(512)S(1)}, f32[512]{0:T(512)}, u32[]{:S(2)}) copy-start(f32[512]{0:T(512)} %param.10) | copy-start | bytes 6148
  45.6 132.8 %all-to-all-start = ((bf16[512,4,1408]{2,0,1:T(8,128)(2,1)}), bf16[512,4,1408]{2,0,1:T(8,128)(2,1)}, u32[]{:S(2)}, u32[]{:S(2)}) async-start(bf16[512,4,1408]{2,0,1:T(8,128)(2,1)} %fusion.1), calls=%async_computation | async-start | bytes 11534336 | tf_op jit(solution)/shard_map/all_to_all | solution.py:28
  178.4 131.5 %all-to-all-start.2 = ((bf16[4,1408,512]{2,1,0:T(8,128)(2,1)}), bf16[4,1408,512]{2,1,0:T(8,128)(2,1)}, u32[]{:S(2)}, u32[]{:S(2)}) async-start(bf16[4,1408,512]{2,1,0:T(8,128)(2,1)} %bitcast.58), calls=%async_computation.2 | async-start | bytes 11534336 | tf_op jit(solution)/shard_map/all_to_all | solution.py:31
  309.9 131.6 %all-to-all-start.1 = ((bf16[4,512,1408]{2,1,0:T(8,128)(2,1)}), bf16[4,512,1408]{2,1,0:T(8,128)(2,1)}, u32[]{:S(2)}, u32[]{:S(2)}) async-start(bf16[4,512,1408]{2,1,0:T(8,128)(2,1)} %pad_maximum_fusion), calls=%async_computation.1 | async-start | bytes 11534336 | tf_op jit(solution)/shard_map/all_to_all | solution.py:12
  315.1 215.8 %reduce-scatter.2.cloned.1.call-start = ((), (), s32[]{:S(2)}) async-start(), calls=%async_computation.6 | async-start | bytes 5242880 | tf_op jit(solution)/shard_map/reduce_scatter | solution.py:61
  455.4 81.0 %copy-start.1 = (f32[192,2]{0,1:T(2,128)S(1)}, f32[192,2]{0,1:T(2,128)}, u32[]{:S(2)}) copy-start(f32[192,2]{0,1:T(2,128)} %param.9) | copy-start | bytes 4612
  533.0 12.3 %all-to-all-start.4 = ((bf16[4,128,512]{2,1,0:T(8,128)(2,1)}), bf16[4,128,512]{2,1,0:T(8,128)(2,1)S(1)}, u32[]{:S(2)}, u32[]{:S(2)}) async-start(bf16[4,128,512]{2,1,0:T(8,128)(2,1)} %bitcast.17), calls=%async_computation.5 | async-start | bytes 1048576 | tf_op jit(solution)/shard_map/all_to_all | solution.py:64
Sparse Core Ops, SparseCore 0:
  455.6 75.2 reduce-scatter.1
